TPU v7x, 128 devices: a whole 4x4x4 slice. The times are simulated.
128 devices in a mesh: sp: 32 (over z, y, core), tp: 4 (over x).
Axes of the slice: x: 4, y: 4, z: 4, core: 2. Of those that a mesh axis runs over, the one named last changes fastest.
Arguments:
- queries: bfloat16 [24576, 1024], P('sp', 'tp'), may hold values from -6 to 6
- keys: bfloat16 [24576, 1024], P('sp', 'tp'), may hold values from -6 to 6
- values: bfloat16 [24576, 2048], P('sp', 'tp'), may hold values from -6 to 6
- out_gate: bfloat16 [24576, 2048], P('sp', 'tp'), may hold values from -6 to 6
- input_gates: float32 [2, 4, 24576], P(None, 'tp', 'sp'), may hold values from -4 to 300
- forget_gates: float32 [2, 4, 24576], P(None, 'tp', 'sp'), may hold values from -1 to 16
- doc_ids: int32 [24576], P('sp'), may hold values from 0 to 15, never falling along the last dimension, each value on 1 to 3072 neighbouring positions
- head_gain: float32 [2048], P('tp'), may hold values from 0.1 to 1.9
- w_out: bfloat16 [2048, 2048], P('tp'), may hold values from -0.25 to 0.25
- resid: bfloat16 [24576, 2048], P(('sp', 'tp')), may hold values from -30 to 30
- norm_gain: float32 [2048], replicated, may hold values from 0.1 to 1.9
- w_up: bfloat16 [2048, 8192], P('sp', 'tp'), may hold values from -0.125 to 0.125
- w_down: bfloat16 [8192, 2048], P('tp', 'sp'), may hold values from -0.0625 to 0.0625
Outputs:
- layer_out: bfloat16 [24576, 2048], P(('sp', 'tp'))
Inputs may be any that keep to these rules, and one draw needn't show every extreme that they name: `doc_ids`: document numbers never fall along the positions.
All inputs are finite; a program needn't handle non-finite values.
Results may differ from a plain program's by a relative error of at most 0.013.
Values may be sent and summed in bfloat16 or wider, within the bound.
A program may use at most 128 MiB of HBM per device.

v0:
```python
import jax
import jax.numpy as jnp
from jax import lax
from jax.sharding import Mesh
from jax.sharding import PartitionSpec as P

SP = ("sp_0", "sp_1", "sp_2")
SP_TP = ("sp_0", "sp_1", "sp_2", "tp")
eps = 1e-06
far_low = -1e30


def neutral_like(value, identity):
    return jax.tree.map(
        lambda a, e: jnp.broadcast_to(jnp.asarray(e, a.dtype), a.shape), value, identity
    )


def gathered_once(value, axis):
    leaves = jax.tree.leaves(value)
    turns = sorted(range(len(leaves)), key=lambda k: -leaves[k].size)
    width = (1, *leaves[turns[0]].shape)[-1]
    lines = [
        jnp.pad(leaves[k].reshape(-1), (0, -leaves[k].size % width)).reshape(-1, width)
        for k in turns
    ]
    both, at, found = (lax.all_gather(jnp.concatenate(lines), axis), 0, {})
    for k, line in zip(turns, lines):
        section = both[:, at : at + len(line)].reshape(len(both), -1)
        found[k] = section[:, : leaves[k].size].reshape(-1, *leaves[k].shape)
        at += len(line)
    numbers = iter(range(len(leaves)))
    return jax.tree.map(lambda _: found[next(numbers)], value)


def carried_in(value, axes, combine, identity, reverse):
    before = start = neutral_like(value, identity)
    running = value
    for axis in reversed(axes):
        length, index = (lax.axis_size(axis), lax.axis_index(axis))
        pieces = gathered_once(
            jax.tree.map(
                lambda part, kind: part.astype(kind),
                running,
                jax.tree.map(lambda a: jnp.bfloat16 if a.dtype == jnp.float32 else a.dtype, value),
            ),
            axis,
        )
        inside, running = (start, start)
        for k in reversed(range(length)) if reverse else range(length):
            passed = k > index if reverse else k < index
            running = combine(
                running, jax.tree.map(lambda part, own: part[k].astype(own.dtype), pieces, value)
            )
            inside = jax.tree.map(lambda new, old: jnp.where(passed, new, old), running, inside)
        before = combine(inside, before)
    return before


def split_up(value, dim, length):
    dims = value.shape
    pieces = value.reshape(*dims[:dim], length, dims[dim] // length, *dims[dim + 1 :])
    return jnp.moveaxis(pieces, dim, 0)


def sent_and_summed(value, axis, dim):
    length = lax.axis_size(axis)
    pieces = lax.all_to_all(split_up(value, dim, length), axis, 0, 0, tiled=True)
    return jnp.sum(pieces.astype(jnp.float32), axis=0)


def summarize(keys_blk, values_blk, in_gate, forget_pre, doc_pos):
    logf = jax.nn.log_sigmoid(forget_pre)
    cum = jnp.cumsum(logf)
    length = keys_blk.shape[0]
    last_doc = doc_pos[length - 1]
    tail = doc_pos == last_doc
    total = cum[length - 1]
    exponent = jnp.where(tail, total - cum + in_gate, far_low)
    peak = jnp.max(exponent)
    scaled = jnp.exp(exponent - peak)
    weighted = (keys_blk * scaled[:, None]).astype(jnp.bfloat16)
    memory = jnp.einsum("sd,sv->dv", weighted, values_blk, preferred_element_type=jnp.float32)
    norm_keys = jnp.sum(weighted.astype(jnp.float32), axis=0)
    return (memory, norm_keys, peak, total, doc_pos[0], last_doc, jnp.zeros((), jnp.float32))


def emit(queries_blk, keys_blk, values_blk, in_gate, forget_pre, doc_pos, state):
    memory, norm_keys, top_in, total_in, first_in, last_in, empty_in = state
    scale = queries_blk.shape[1] ** (-0.5)
    logf = jax.nn.log_sigmoid(forget_pre)
    cum = jnp.cumsum(logf)
    length = queries_blk.shape[0]
    place = jnp.arange(length)
    keep = (place[:, None] >= place[None, :]) & (doc_pos[:, None] == doc_pos[None, :])
    exponent = jnp.where(keep, cum[:, None] - cum[None, :] + in_gate[None, :], far_low)
    usable = (doc_pos == last_in) & (empty_in < 0.5)
    carried = jnp.where(usable, cum + top_in, far_low)
    peak = jnp.maximum(carried, jnp.max(exponent, axis=1))
    scores = (
        jnp.einsum("td,sd->ts", queries_blk, keys_blk, preferred_element_type=jnp.float32) * scale
    )
    weights = jnp.where(keep, scores * jnp.exp(exponent - peak[:, None]), 0.0)
    inter = jnp.where(usable, jnp.exp(carried - peak), 0.0)
    query_wide = queries_blk.astype(jnp.float32)
    numer = jnp.dot(weights.astype(jnp.bfloat16), values_blk, preferred_element_type=jnp.float32)
    numer = numer + (inter * scale)[:, None] * jnp.dot(query_wide, memory)
    denom = jnp.sum(weights, axis=1) + inter * scale * jnp.dot(query_wide, norm_keys)
    return numer / jnp.maximum(jnp.abs(denom), 1.0)[:, None]


def combine(early, late):
    e_mem, e_keys, e_top, e_total, e_first, e_last, e_empty = early
    l_mem, l_keys, l_top, l_total, l_first, l_last, l_empty = late
    linked = (l_first == e_last) & (l_first == l_last) & (e_empty < 0.5)
    top = jnp.where(linked, jnp.maximum(l_top, e_top + l_total), l_top)
    early_part = jnp.where(linked, jnp.exp(jnp.minimum(e_top + l_total - top, 0.0)), 0.0)
    late_part = jnp.exp(l_top - top)
    joined = (
        early_part * e_mem + late_part * l_mem,
        early_part * e_keys + late_part * l_keys,
        top,
        e_total + l_total,
        jnp.where(e_empty > 0.5, l_first, e_first),
        l_last,
        jnp.zeros_like(l_empty),
    )
    return tuple((jnp.where(l_empty > 0.5, a, b) for a, b in zip(early, joined)))


def direction(queries3, keys3, values3, in_gates, forget_pre, doc_pos, backward):
    if backward:
        queries3, keys3, values3 = (queries3[::-1], keys3[::-1], values3[::-1])
        in_gates, forget_pre, doc_pos = (in_gates[:, ::-1], forget_pre[:, ::-1], doc_pos[::-1])
    summary = jax.vmap(summarize, in_axes=(1, 1, 0, 0, None))(
        keys3, values3, in_gates, forget_pre, doc_pos
    )
    heads = in_gates.shape[0]
    start = (
        jnp.zeros((heads, keys3.shape[2], values3.shape[2]), jnp.float32),
        jnp.zeros((heads, keys3.shape[2]), jnp.float32),
        jnp.full((heads,), far_low, jnp.float32),
        jnp.zeros((heads,), jnp.float32),
        jnp.full((heads,), -1.0, jnp.float32),
        jnp.full((heads,), -1.0, jnp.float32),
        jnp.ones((heads,), jnp.float32),
    )
    if backward:
        incoming = carried_in(summary, SP, jax.vmap(combine), start, True)
    else:
        incoming = carried_in(summary, SP, jax.vmap(combine), start, False)
    result = jax.vmap(emit, in_axes=(1, 1, 1, 0, 0, None, 0), out_axes=1)(
        queries3, keys3, values3, in_gates, forget_pre, doc_pos, incoming
    )
    if backward:
        result = result[::-1]
    return result


def fetch_weights(w_up, w_down):
    up_full = lax.all_gather(w_up, SP, axis=0, tiled=True)
    down_full = lax.all_gather(w_down, SP, axis=1, tiled=True)
    return (up_full, down_full)


def rms_scale(mixed, norm_gain):
    factor = lax.rsqrt(jnp.mean(mixed * mixed, axis=-1, keepdims=True) + eps)
    return (mixed * factor * norm_gain).astype(jnp.bfloat16)


def shards(
    queries,
    keys,
    values,
    out_gate,
    input_gates,
    forget_gates,
    doc_ids,
    head_gain,
    w_out,
    resid,
    norm_gain,
    w_up,
    w_down,
):
    length = queries.shape[0]
    heads = input_gates.shape[1]
    queries3 = queries.reshape(length, heads, -1)
    keys3 = keys.reshape(length, heads, -1)
    values3 = values.reshape(length, heads, -1)
    doc_pos = doc_ids.astype(jnp.float32)
    memory = direction(queries3, keys3, values3, input_gates[0], forget_gates[0], doc_pos, False)
    memory = memory + direction(
        queries3, keys3, values3, input_gates[1], forget_gates[1], doc_pos, True
    )
    normed = memory * lax.rsqrt(jnp.mean(memory * memory, axis=-1, keepdims=True) + eps)
    gate = jax.nn.sigmoid(out_gate.astype(jnp.float32)).reshape(length, heads, -1)
    readout = (
        (normed * head_gain.reshape(heads, -1) * gate).astype(jnp.bfloat16).reshape(length, -1)
    )
    up_full, down_full = fetch_weights(w_up, w_down)
    picked = readout
    mixed = resid.astype(jnp.float32) + sent_and_summed(
        jnp.dot(picked, w_out, preferred_element_type=jnp.float32).astype(jnp.bfloat16), "tp", 0
    )
    scaled = rms_scale(mixed, norm_gain)
    product = jnp.dot(
        lax.all_gather(scaled, "tp", axis=0, tiled=True),
        up_full,
        preferred_element_type=jnp.float32,
    )
    hidden = jnp.square(jax.nn.relu(product)).astype(jnp.bfloat16)
    picked = hidden
    return (
        mixed
        + sent_and_summed(
            jnp.dot(picked, down_full, preferred_element_type=jnp.float32).astype(jnp.bfloat16),
            "tp",
            0,
        )
    ).astype(jnp.bfloat16)


def solution(mesh):
    split = Mesh(mesh.devices.reshape(4, 4, 2, mesh.shape["tp"]), ("sp_0", "sp_1", "sp_2", "tp"))
    return jax.shard_map(
        shards,
        mesh=split,
        in_specs=(
            P(SP, "tp"),
            P(SP, "tp"),
            P(SP, "tp"),
            P(SP, "tp"),
            P(None, "tp", SP),
            P(None, "tp", SP),
            P(SP),
            P("tp"),
            P("tp", None),
            P(SP_TP, None),
            P(),
            P(SP, "tp"),
            P("tp", SP),
        ),
        out_specs=P(SP_TP, None),
        check_vma=False,
    )
```

profile of v0, /device:TPU:0, one launch (start us, length us, event | category | flops | bytes accessed | tf_op | source)
XLA Modules:
  0.0 496.2 jit_solution(1414788614506800733)
XLA Ops:
  6.5 0.9 negate_reduce_fusion
  8.8 0.7 slice.962
  9.4 0.7 convert_element_type.975
  10.7 0.7 slice_reduce_fusion.2
  13.3 2.1 fusion.304
  16.0 0.6 subtract_exponential_fusion
  16.6 1.2 fusion.204
  17.8 1.9 convolution_convert_fusion.3
  20.6 2.2 all-gather.6
  37.3 1.4 concatenate.19
  38.8 3.8 reverse.15
  42.7 11.9 %reverse.16 = bf16[768,512]{1,0:T(8,128)(2,1)} reverse(bf16[768,512]{1,0:T(8,128)(2,1)} %param.15), dimensions={0} | reverse | bytes 1572864 | tf_op jit(solution)/shard_map/reverse.3
  58.3 1.3 fusion.305
  60.2 0.6 exponential_reduce_fusion
  60.9 1.2 fusion.205
  62.0 1.8 convolution_convert_fusion.2
  64.1 2.2 all-gather.9
  80.7 1.4 concatenate.22
  82.2 1.1 fusion.307
  111.6 1.5 fusion.146
  113.1 1.4 concatenate.20
  114.6 1.1 fusion.309
  144.4 1.5 fusion.147
  145.9 1.4 concatenate.23
  147.7 6.3 %reverse.14 = bf16[768,256]{1,0:T(8,128)(2,1)} reverse(bf16[768,256]{1,0:T(8,128)(2,1)} %param.13), dimensions={0} | reverse | bytes 786432 | tf_op jit(solution)/shard_map/reverse
  154.0 2.3 copy.540
  158.0 1.1 fusion.306
  182.1 1.1 fusion.308
  206.5 2.1 fusion.344
  208.6 2.0 fusion.9
  211.5 1.5 fusion.343
  213.0 0.8 fusion.7
  214.2 4.4 fusion.4
  218.5 13.6 %reverse.17 = f32[768,512]{0,1:T(8,128)} reverse(f32[768,512]{0,1:T(8,128)} %fusion.4), dimensions={0} | reverse | bytes 3145728 | tf_op jit(solution)/shard_map/reverse.5
  232.4 4.4 multiply_reduce_fusion.1
  236.8 2.0 convolution_convert_fusion.1
  238.8 42.3 %all_to_all.10 = bf16[4,192,2048]{2,1,0:T(8,128)(2,1)S(1)} all-to-all(bf16[4,192,2048]{2,1,0:T(8,128)(2,1)S(1)} %bitcast.464), channel_id=1, replica_groups=mesh['sp_0'=4,'sp_1'=4,'sp_2'=2,'tp'=4] {'tp'}, dimensions={0} | all-to-all | bytes 6291456 | tf_op jit(solution)/shard_map/all_to_all | solution.py:68
  282.5 0.8 copy-done.2
  283.4 1.1 multiply_convert_fusion.1
  285.1 0.7 all-gather.24.cloned.1.call-update
  285.8 38.8 %all-gather.20.cloned.1.call-done = bf16[768,2048]{1,0:T(8,128)(2,1)} async-done(((bf16[192,2048]{1,0:T(8,128)(2,1)}), bf16[768,2048]{1,0:T(8,128)(2,1)}) %all-gather.20.cloned.1.call-update) | async-done | bytes 3145744 | tf_op jit(solution)/shard_map/all_gather | solution.py:208
  324.7 55.2 %all-gather.22.cloned.1.call-done = bf16[2048,2048]{1,0:T(8,128)(2,1)} async-done(((bf16[64,2048]{1,0:T(8,128)(2,1)}), bf16[2048,2048]{1,0:T(8,128)(2,1)}) %all-gather.22.cloned.1.call-update) | async-done | bytes 8388624 | tf_op jit(solution)/shard_map/all_gather | solution.py:161
  379.9 11.9 %multiply_convert_fusion = bf16[768,2048]{1,0:T(8,128)(2,1)} fusion(bf16[768,2048]{1,0:T(8,128)(2,1)} %all-gather.20.cloned.1.call-done, bf16[2048,2048]{1,0:T(8,128)(2,1)} %all-gather.22.cloned.1.call-done), kind=kOutput, calls=%fused_computation.1 | convolution fusion | flops 6447169536 | bytes 14680064 | tf_op jit(solution)/shard_map/dot_general | solution.py:207
  391.8 42.8 %all-gather.24.cloned.1.call-done = bf16[2048,2048]{0,1:T(8,128)(2,1)} async-done(((bf16[2048,64]{0,1:T(8,128)(2,1)}), bf16[2048,2048]{0,1:T(8,128)(2,1)}) %all-gather.24.cloned.1.call-update) | async-done | bytes 8388624 | tf_op jit(solution)/shard_map/all_gather | solution.py:162
  434.5 10.1 %convolution_convert_fusion = bf16[768,2048]{1,0:T(8,128)(2,1)S(1)} fusion(bf16[768,2048]{1,0:T(8,128)(2,1)} %multiply_convert_fusion, bf16[2048,2048]{0,1:T(8,128)(2,1)} %all-gather.24.cloned.1.call-done), kind=kOutput, calls=%fused_computation.3 | convolution fusion | flops 6444023808 | bytes 14680064 | tf_op jit(solution)/shard_map/dot_general | solution.py:217
  444.6 42.0 %all_to_all.11 = bf16[4,192,2048]{2,1,0:T(8,128)(2,1)S(1)} all-to-all(bf16[4,192,2048]{2,1,0:T(8,128)(2,1)S(1)} %bitcast.465), channel_id=1, replica_groups=mesh['sp_0'=4,'sp_1'=4,'sp_2'=2,'tp'=4] {'tp'}, dimensions={0} | all-to-all | bytes 6291456 | tf_op jit(solution)/shard_map/all_to_all | solution.py:68
  487.3 0.8 copy-done.3
  488.1 1.2 add_convert_fusion
  (216 shorter events, 28.4 us)
Async XLA Ops:
  6.5 230.3 %copy-start = (bf16[512,2048]{1,0:T(8,128)(2,1)S(1)}, bf16[512,2048]{1,0:T(8,128)(2,1)}, u32[]{:S(2)}) copy-start(bf16[512,2048]{1,0:T(8,128)(2,1)} %param.21) | copy-start | bytes 6291460
  6.5 75.6 %all-gather.26.cloned.1.call-start = ((), (), s32[]{:S(2)}) async-start(), calls=%async_computation.5 | async-start | bytes 1351680 | tf_op jit(solution)/shard_map/all_gather | solution.py:27
  17.8 21.0 %copy-start.5 = (bf16[768,256]{1,0:T(8,128)(2,1)S(1)}, bf16[768,256]{1,0:T(8,128)(2,1)}, u32[]{:S(2)}) copy-start(bf16[768,256]{1,0:T(8,128)(2,1)} %param.14) | copy-start | bytes 1179652
  38.7 75.9 %all-gather.30.cloned.1.call-start = ((), (), s32[]{:S(2)}) async-start(), calls=%async_computation.7 | async-start | bytes 1351680 | tf_op jit(solution)/shard_map/all_gather | solution.py:27
  82.1 75.9 %all-gather.28.cloned.1.call-start = ((), (), s32[]{:S(2)}) async-start(), calls=%async_computation.6 | async-start | bytes 1351680 | tf_op jit(solution)/shard_map/all_gather | solution.py:27
  114.5 67.6 %all-gather.32.cloned.1.call-start = ((), (), s32[]{:S(2)}) async-start(), calls=%async_computation.8 | async-start | bytes 1351680 | tf_op jit(solution)/shard_map/all_gather | solution.py:27
  145.9 60.5 %copy-start.12 = (s32[768]{0:T(1024)S(1)}, s32[768]{0:T(1024)}, u32[]{:S(2)}) copy-start(s32[768]{0:T(1024)} %param.19) | copy-start | bytes 9220
  147.3 177.3 %all-gather.20.cloned.1.call-start = ((), (), s32[]{:S(2)}) async-start(), calls=%async_computation.2 | async-start | bytes 3932160 | tf_op jit(solution)/shard_map/all_gather | solution.py:208
  206.5 2.1 copy-start.9
  208.6 2.9 copy-start.7
  208.6 2.9 copy-start.8
  211.5 1.5 copy-start.10
  218.5 13.6 %copy-start.6 = (bf16[768,256]{1,0:T(8,128)(2,1)S(1)}, bf16[768,256]{1,0:T(8,128)(2,1)}, u32[]{:S(2)}) copy-start(bf16[768,256]{1,0:T(8,128)(2,1)} %param.13) | copy-start | bytes 1179652
  232.4 4.4 copy-start.11
  232.4 4.4 copy-start.14
  281.1 1.1 copy-start.4
  282.2 1.1 copy-start.2
  282.2 1.1 copy-start.13
  284.5 95.4 %all-gather.22.cloned.1.call-start = ((), (), s32[]{:S(2)}) async-start(), calls=%async_computation.3 | async-start | bytes 8650752 | tf_op jit(solution)/shard_map/all_gather | solution.py:161
  285.1 149.5 %all-gather.24.cloned.1.call-start = ((), (), s32[]{:S(2)}) async-start(), calls=%async_computation.4 | async-start | bytes 8650752 | tf_op jit(solution)/shard_map/all_gather | solution.py:162
  486.7 1.4 copy-start.3
  486.7 2.6 copy-start.1
Sparse Core Ops, SparseCore 0:
  38.8 26.7 all-gather.25
  82.2 26.6 all-gather.29
  114.6 26.8 all-gather.27
  147.5 26.8 all-gather.31
  284.6 39.9 all-gather.19
  326.8 53.0 all-gather.21
  382.1 52.3 all-gather.23
where the time goes:
time: 502 us; the launch traced here: 496 us
  waiting for transfers between devices  138 us (27%)
  between operations  134 us (27%)
  blocking collectives  88.7 us (18%)
  local copies, waits for them, and re-layouts  72.9 us (15%)
  matrix products  43.3 us (9%)
  other arithmetic  18.8 us (4%)
    all_to_all x2, blocking collectives, sent_and_summed(): lax.all_to_all(split_up(value, dim, length), axis, 0, 0, tiled=True)  84.3 us
    all_gather x1, waiting for transfers between devices, fetch_weights(): up_full = lax.all_gather(w_up, SP, axis=0, tiled=True)  55.2 us
    all_gather x1, waiting for transfers between devices, fetch_weights(): down_full = lax.all_gather(w_down, SP, axis=1, tiled=True)  42.8 us
    all_gather x1, waiting for transfers between devices, shards(): lax.all_gather(scaled, 'tp', axis=0, tiled=True)  38.8 us
    another operation x7, local copies, waits for them, and re-layouts  35.8 us
    slice x30, local copies, waits for them, and re-layouts, carried_in(): part[k].astype(own.dtype)  17.1 us
    dot_general x1, matrix products, shards(): jnp.dot(lax.all_gather(scaled, 'tp', axis=0, tiled=True), up_full, prefer...  11.9 us
    dot_general x1, matrix products, shards(): jnp.dot(picked, down_full, preferred_element_type=jnp.float32)  10.1 us
  transfers between devices with their start and end apart: 7, of which 3 were waited for; matrix products, arithmetic and copies ran while one was open for 14% of the time, Pallas kernels for 0%

commit v1 on v0

--- a/solution.py
+++ b/solution.py
@@ -204,11 +204,20 @@
         jnp.dot(picked, w_out, preferred_element_type=jnp.float32).astype(jnp.bfloat16), "tp", 0
     )
     scaled = rms_scale(mixed, norm_gain)
-    product = jnp.dot(
-        lax.all_gather(scaled, "tp", axis=0, tiled=True),
-        up_full,
-        preferred_element_type=jnp.float32,
-    )
+
+    def signs_meet(page):
+        ax_name = "tp"
+        workers = lax.axis_size(ax_name)
+        e_next = lax.all_to_all(
+            jnp.tile(page, [workers if it == 0 else 1 for it in range(page.ndim)]),
+            ax_name,
+            split_axis=0,
+            concat_axis=0,
+            tiled=True,
+        )
+        return e_next
+
+    product = jnp.dot(signs_meet(scaled), up_full, preferred_element_type=jnp.float32)
     hidden = jnp.square(jax.nn.relu(product)).astype(jnp.bfloat16)
     picked = hidden
     return (

time: 502 us -> 405 us (0.81)
  waiting for transfers between devices: 138 us -> 1.2 us
  blocking collectives: 88.7 us -> 125 us
    all_gather x1, waiting for transfers between devices: 55.2 us -> 0.01 us  [fetch_weights(): up_full = lax.all_gather(w_up, SP, axis=0, tiled=True)]
    all_gather x1, waiting for transfers between devices: 42.8 us -> 0.01 us  [fetch_weights(): down_full = lax.all_gather(w_down, SP, axis=1, tiled=True)]
    all_to_all x0 -> x1, blocking collectives: none -> 40.1 us  [signs_meet(): lax.all_to_all(jnp.tile(page, [workers if it == 0 else 1 for it in range(...]
    all_gather x1 -> x0, waiting for transfers between devices: 38.8 us -> none  [shards(): lax.all_gather(scaled, 'tp', axis=0, tiled=True)]
    another operation x7 -> x8, local copies, waits for them, and re-layouts: 35.8 us -> 36.4 us
  transfers between devices with their start and end apart: 7 -> 6, of which waited for: 3 -> 0; matrix products, arithmetic and copies ran while one was open for 14% -> 27% of each run, Pallas kernels for 0% -> 0%
where the time goes in v1:
time: 405 us; the launch traced here: 398 us
  between operations  136 us (34%)
  blocking collectives  125 us (31%)
  local copies, waits for them, and re-layouts  74.3 us (18%)
  matrix products  44.2 us (11%)
  other arithmetic  17.6 us (4%)
    all_to_all x2, blocking collectives, sent_and_summed(): lax.all_to_all(split_up(value, dim, length), axis, 0, 0, tiled=True)  80.6 us
    all_to_all x1, blocking collectives, signs_meet(): lax.all_to_all(jnp.tile(page, [workers if it == 0 else 1 for it in range(...  40.1 us
    another operation x7, local copies, waits for them, and re-layouts  36 us
    slice x30, local copies, waits for them, and re-layouts, carried_in(): part[k].astype(own.dtype)  17.4 us
    dot_general x1, matrix products, shards(): jnp.dot(signs_meet(scaled), up_full, preferred_element_type=jnp.float32)  11.9 us
    dot_general x1, matrix products, shards(): jnp.dot(picked, down_full, preferred_element_type=jnp.float32)  10.1 us
  transfers between devices with their start and end apart: 6, of which 0 were waited for; matrix products, arithmetic and copies ran while one was open for 27% of the time, Pallas kernels for 0%

profile of v1, /device:TPU:0, one launch (start us, length us, event | category | flops | bytes accessed | tf_op | source)
XLA Modules:
  0.0 398.1 jit_solution(3723046107489536877)
XLA Ops:
  6.5 0.9 negate_reduce_fusion
  8.8 0.7 slice.962
  9.4 0.7 convert_element_type.975
  10.7 0.7 slice_reduce_fusion.2
  13.3 2.0 fusion.304
  16.5 1.2 fusion.204
  17.6 1.9 convolution_convert_fusion.3
  20.3 2.2 all-gather.6
  37.1 1.4 concatenate.19
  38.6 3.8 reverse.15
  42.5 11.9 %reverse.16 = bf16[768,512]{1,0:T(8,128)(2,1)} reverse(bf16[768,512]{1,0:T(8,128)(2,1)} %param.15), dimensions={0} | reverse | bytes 1572864 | tf_op jit(solution)/shard_map/reverse.3
  58.0 1.2 fusion.305
  60.3 1.2 fusion.205
  61.5 1.8 convolution_convert_fusion.2
  63.5 2.2 all-gather.9
  80.7 1.4 concatenate.22
  82.2 1.3 fusion.307
  87.1 0.6 fusion.317
  94.0 0.6 fusion.318
  112.2 1.5 fusion.146
  113.7 1.4 concatenate.20
  115.2 1.1 fusion.309
  145.3 1.5 fusion.147
  146.8 1.4 concatenate.23
  149.5 6.5 %reverse.14 = bf16[768,256]{1,0:T(8,128)(2,1)} reverse(bf16[768,256]{1,0:T(8,128)(2,1)} %param.13), dimensions={0} | reverse | bytes 786432 | tf_op jit(solution)/shard_map/reverse
  156.0 2.3 copy.540
  159.0 0.6 select_reduce_fusion
  160.0 1.1 fusion.306
  161.1 0.6 fusion.316
  184.3 1.1 fusion.308
  186.8 0.6 fusion.323
  210.2 1.3 convolution_reduce_fusion
  211.5 2.1 fusion.343
  213.6 0.8 fusion.7
  214.6 4.3 %fusion.4 = f32[768,512]{0,1:T(8,128)} fusion(f32[768,512]{0,1:T(8,128)S(1)} %fusion.7, bf16[768,256]{1,0:T(8,128)(2,1)S(1)} %copy-done.9, f32[768]{0:T(1024)S(1)} %get-tuple-element.16, f32[768]{0:T(1024)S(1)} %get-tuple-element.17, bf16[4,262,512]{2,1,0:T(8,128)(2,1)} %all-gather.29.cloned.1.call-done, f32[]{:T(128)} %bitcast.267, f32[]{:T(128)} %bitcast.266, ...), kind=kOutput, calls=%fused_computation.16 | convolution fusion | flops 210632704 | bytes 6190592 | tf_op jit(solution)/shard_map/vmap()/dot_general | solution.py:107
  218.9 13.6 %reverse.17 = f32[768,512]{0,1:T(8,128)} reverse(f32[768,512]{0,1:T(8,128)} %fusion.4), dimensions={0} | reverse | bytes 3145728 | tf_op jit(solution)/shard_map/reverse.5
  232.5 1.3 convolution_reduce_fusion.1
  233.8 2.6 fusion.344
  236.5 0.8 fusion.9
  237.9 3.4 multiply_reduce_fusion.1
  241.4 2.0 convolution_convert_fusion.1
  243.3 42.1 %all_to_all.19 = bf16[4,192,2048]{2,1,0:T(8,128)(2,1)S(1)} all-to-all(bf16[4,192,2048]{2,1,0:T(8,128)(2,1)S(1)} %bitcast.466), channel_id=1, replica_groups=mesh['sp_0'=4,'sp_1'=4,'sp_2'=2,'tp'=4] {'tp'}, dimensions={0} | all-to-all | bytes 6291456 | tf_op jit(solution)/shard_map/all_to_all | solution.py:68
  288.2 40.1 %all_to_all.20 = bf16[4,192,2048]{2,1,0:T(8,128)(2,1)} all-to-all(bf16[4,192,2048]{2,1,0:T(8,128)(2,1)S(1)} %tile.2), channel_id=1, replica_groups=mesh['sp_0'=4,'sp_1'=4,'sp_2'=2,'tp'=4] {'tp'}, dimensions={0} | all-to-all | bytes 6291456 | tf_op jit(solution)/shard_map/all_to_all | solution.py:211
  328.2 11.9 %multiply_convert_fusion = bf16[768,2048]{1,0:T(8,128)(2,1)} fusion(bf16[768,2048]{1,0:T(8,128)(2,1)} %bitcast.465, bf16[2048,2048]{1,0:T(8,128)(2,1)} %all-gather.19.cloned.1.call-done), kind=kOutput, calls=%fused_computation.1 | convolution fusion | flops 6447169536 | bytes 14680064 | tf_op jit(solution)/shard_map/dot_general | solution.py:220
  340.1 10.1 %convolution_convert_fusion = bf16[768,2048]{1,0:T(8,128)(2,1)S(1)} fusion(bf16[768,2048]{1,0:T(8,128)(2,1)} %multiply_convert_fusion, bf16[2048,2048]{0,1:T(8,128)(2,1)} %all-gather.21.cloned.1.call-done), kind=kOutput, calls=%fused_computation.3 | convolution fusion | flops 6444023808 | bytes 14680064 | tf_op jit(solution)/shard_map/dot_general | solution.py:226
  350.2 38.4 %all_to_all.21 = bf16[4,192,2048]{2,1,0:T(8,128)(2,1)S(1)} all-to-all(bf16[4,192,2048]{2,1,0:T(8,128)(2,1)S(1)} %bitcast.467), channel_id=1, replica_groups=mesh['sp_0'=4,'sp_1'=4,'sp_2'=2,'tp'=4] {'tp'}, dimensions={0} | all-to-all | bytes 6291456 | tf_op jit(solution)/shard_map/all_to_all | solution.py:68
  389.2 0.8 copy-done.3
  390.0 1.2 add_convert_fusion
  (217 shorter events, 28.4 us)
Async XLA Ops:
  6.5 234.8 %copy-start = (bf16[512,2048]{1,0:T(8,128)(2,1)S(1)}, bf16[512,2048]{1,0:T(8,128)(2,1)}, u32[]{:S(2)}) copy-start(bf16[512,2048]{1,0:T(8,128)(2,1)} %param.21) | copy-start | bytes 6291460
  6.5 75.6 %all-gather.23.cloned.1.call-start = ((), (), s32[]{:S(2)}) async-start(), calls=%async_computation.5 | async-start | bytes 1351680 | tf_op jit(solution)/shard_map/all_gather | solution.py:27
  17.6 21.0 %copy-start.6 = (bf16[768,256]{1,0:T(8,128)(2,1)S(1)}, bf16[768,256]{1,0:T(8,128)(2,1)}, u32[]{:S(2)}) copy-start(bf16[768,256]{1,0:T(8,128)(2,1)} %param.14) | copy-start | bytes 1179652
  38.5 76.7 %all-gather.27.cloned.1.call-start = ((), (), s32[]{:S(2)}) async-start(), calls=%async_computation.7 | async-start | bytes 1351680 | tf_op jit(solution)/shard_map/all_gather | solution.py:27
  82.1 77.9 %all-gather.25.cloned.1.call-start = ((), (), s32[]{:S(2)}) async-start(), calls=%async_computation.6 | async-start | bytes 1351680 | tf_op jit(solution)/shard_map/all_gather | solution.py:27
  115.1 69.2 %all-gather.29.cloned.1.call-start = ((), (), s32[]{:S(2)}) async-start(), calls=%async_computation.8 | async-start | bytes 1351680 | tf_op jit(solution)/shard_map/all_gather | solution.py:27
  148.2 180.0 %all-gather.19.cloned.1.call-start = ((), (), s32[]{:S(2)}) async-start(), calls=%async_computation.3 | async-start | bytes 8650752 | tf_op jit(solution)/shard_map/all_gather | solution.py:161
  148.8 191.3 %all-gather.21.cloned.1.call-start = ((), (), s32[]{:S(2)}) async-start(), calls=%async_computation.4 | async-start | bytes 8650752 | tf_op jit(solution)/shard_map/all_gather | solution.py:162
  211.5 2.1 copy-start.11
  213.6 1.0 copy-start.9
  218.9 14.9 %copy-start.13 = (s32[768]{0:T(1024)S(1)}, s32[768]{0:T(1024)}, u32[]{:S(2)}) copy-start(s32[768]{0:T(1024)} %param.19) | copy-start | bytes 9220
  218.9 14.9 %copy-start.7 = (bf16[768,256]{1,0:T(8,128)(2,1)S(1)}, bf16[768,256]{1,0:T(8,128)(2,1)}, u32[]{:S(2)}) copy-start(bf16[768,256]{1,0:T(8,128)(2,1)} %param.14) | copy-start | bytes 1179652
  233.8 2.6 copy-start.10
  236.5 1.4 copy-start.5
  236.5 1.5 copy-start.8
  237.9 3.4 copy-start.12
  237.9 3.4 copy-start.15
  285.5 1.1 copy-start.4
  286.6 1.1 copy-start.2
  286.6 0.7 copy-start.14
  388.6 1.4 copy-start.3
  388.6 2.6 copy-start.1
Sparse Core Ops, SparseCore 0:
  38.6 26.7 all-gather.22
  82.2 26.6 all-gather.26
  115.2 26.8 all-gather.24
  148.3 26.8 all-gather.28
  177.3 53.1 all-gather.18
  232.6 52.3 all-gather.20
